TPU v7x, 256 devices: a whole 4x4x8 slice. The times are simulated.
256 devices in a mesh: sp: 32 (over z, y), tp: 8 (over x, core).
Axes of the slice: x: 4, y: 4, z: 8, core: 2. Of those that a mesh axis runs over, the one named last changes fastest.
Arguments:
- latent: bfloat16 [16384, 4096], P(('sp', 'tp')), may hold values from -3 to 3
- context: bfloat16 [1024, 4096], P('sp'), may hold values from -6 to 6
- cond: float32 [4096], replicated, may hold values from -6 to 6
- ctx_cond: float32 [4096], replicated, may hold values from -6 to 6
- w_shift: bfloat16 [4096, 4096], P('sp', 'tp'), may hold values from -0.1875 to 0.1875
- w_scale: bfloat16 [4096, 4096], P('sp', 'tp'), may hold values from -0.09375 to 0.15478516
- w_gate: bfloat16 [4096, 4096], P('sp', 'tp'), may hold values from -0.1875 to 0.1875
- w_query: bfloat16 [4096, 2048], P(None, 'tp'), may hold values from -0.09375 to 0.09375
- key_weight: bfloat16 [4096, 1024], P(None, 'tp'), may hold values from -0.09375 to 0.09375
- value_weight: bfloat16 [4096, 1024], P(None, 'tp'), may hold values from -0.09375 to 0.09375
- w_out: bfloat16 [2048, 4096], P('tp'), may hold values from -0.125 to 0.125
- sink: float32 [16], replicated, may hold values from 4 to 8
Outputs:
- mixed: bfloat16 [16384, 4096], P(('sp', 'tp'))
All inputs are finite; a program needn't handle non-finite values.
Results may differ from a plain program's by a relative error of at most 0.035.
Values may be sent and summed in bfloat16 or wider, within the bound.
A program may use at most 64 MiB of HBM per device.

v0:
```python
import jax
import jax.numpy as jnp
from jax import lax
from jax.sharding import PartitionSpec as P

HEAD_SIZE = 128
WINDOW_SIDE = 128
GRID_WIDTH = 64
EPS = 1e-05
THETA = 10000.0
MASKED = -1e30


def sent_to_all(value, axis):
    length = lax.axis_size(axis)
    return lax.all_to_all(
        jnp.broadcast_to(value[None], (length, *value.shape)), axis, 0, 0, tiled=True
    )


def taken_together(value, axis):
    everything = sent_to_all(value, axis)
    return jnp.sum(everything, axis=0)


def in_one(arrays, axis):
    line, at, done = (jnp.concatenate([a.reshape(-1) for a in arrays]), 0, [])
    subtotal = taken_together(line, axis)
    for a in arrays:
        done.append(subtotal[at : at + a.size].reshape(a.shape))
        at += a.size
    return tuple(done)


def side_by_side(arrays, axis, dim, along):
    widths = [a.shape[along] for a in arrays]
    both = jnp.concatenate(arrays, axis=along)
    filled = lax.all_gather(both, axis, axis=dim, tiled=True)
    return tuple(jnp.split(filled, [sum(widths[:k]) for k in range(1, len(widths))], axis=along))


def in_order(tiles, dim):
    tiles = jnp.moveaxis(tiles, 0, dim)
    lengths = tiles.shape
    return tiles.reshape(*lengths[:dim], lengths[dim] * lengths[dim + 1], *lengths[dim + 2 :])


def gather_directly(value, axis, dim):
    tiles = sent_to_all(value, axis)
    return in_order(tiles, dim)


def with_halo(cells, sides, width):
    for axis, dim in sides:
        count = lax.axis_size(axis)
        ends = count - 1
        head = lax.slice_in_dim(cells, 0, width, axis=dim)
        tail = lax.slice_in_dim(cells, cells.shape[dim] - width, cells.shape[dim], axis=dim)
        cells = jnp.concatenate(
            [
                lax.ppermute(tail, axis, [(i, (i + 1) % count) for i in range(ends)]),
                cells,
                lax.ppermute(head, axis, [((i + 1) % count, i) for i in range(ends)]),
            ],
            axis=dim,
        )
    return cells


def layer_norm(rows):
    values = rows.astype(jnp.float32)
    mean = jnp.mean(values, axis=-1, keepdims=True)
    var = jnp.mean(jnp.square(values - mean), axis=-1, keepdims=True)
    return (values - mean) * lax.rsqrt(var + EPS)


def rotate_half(values, token_position, width):
    half = width // 2
    inverse = THETA ** (-jnp.arange(half, dtype=jnp.float32) * 2.0 / width)
    angle = token_position.astype(jnp.float32)[:, None] * inverse[None, :]
    cosine = jnp.cos(angle)[:, None, :]
    sine = jnp.sin(angle)[:, None, :]
    first = values[..., :half]
    second = values[..., half:]
    return jnp.concatenate(
        [first * cosine - second * sine, second * cosine + first * sine], axis=-1
    )


def axial_rotation(heads, token_position, grid):
    width = heads.shape[-1] // 2
    values = heads.astype(jnp.float32)
    turned = jnp.concatenate(
        [
            rotate_half(values[..., :width], token_position // grid, width),
            rotate_half(values[..., width:], token_position % grid, width),
        ],
        axis=-1,
    )
    return turned.astype(jnp.bfloat16)


def sink_weights(scores, sink_column):
    top = jnp.maximum(jnp.max(scores, axis=-1, keepdims=True), sink_column)
    expo = jnp.exp(scores - top)
    return (expo / (jnp.sum(expo, axis=-1, keepdims=True) + jnp.exp(sink_column - top))).astype(
        jnp.bfloat16
    )


def shards(
    latent,
    context,
    cond,
    ctx_cond,
    w_shift,
    w_scale,
    w_gate,
    w_query,
    key_weight,
    value_weight,
    w_out,
    sink,
):
    sp_count = lax.axis_size("sp")
    sp_index = lax.axis_index("sp")
    tp_index = lax.axis_index("tp")
    block_rows = w_shift.shape[0]
    act = jax.nn.silu(jnp.stack([cond, ctx_cond])).astype(jnp.bfloat16)
    own_act = lax.dynamic_slice_in_dim(act, sp_index * block_rows, block_rows, 1)
    shift_part = jnp.dot(own_act, w_shift, preferred_element_type=jnp.float32)
    scale_part = jnp.dot(own_act, w_scale, preferred_element_type=jnp.float32)
    gate_part = jnp.dot(own_act[0:1], w_gate, preferred_element_type=jnp.float32)
    shift_sum, scale_sum, gate_sum = in_one((shift_part, scale_part, gate_part), "sp")
    shift, scale, gate = side_by_side((shift_sum, scale_sum, gate_sum), "tp", 1, 0)
    latent_mod = (layer_norm(latent) * (1.0 + scale[0]) + shift[0]).astype(jnp.bfloat16)
    ctx_mod = (layer_norm(context) * (1.0 + scale[1]) + shift[1]).astype(jnp.bfloat16)
    kv_cols = key_weight.shape[1]
    q_cols = w_query.shape[1]
    ctx_pair = gather_directly(
        jnp.concatenate(
            [
                jnp.dot(ctx_mod, key_weight, preferred_element_type=jnp.float32).astype(
                    jnp.bfloat16
                ),
                jnp.dot(ctx_mod, value_weight, preferred_element_type=jnp.float32).astype(
                    jnp.bfloat16
                ),
            ],
            axis=1,
        ),
        "sp",
        0,
    )
    piece = lax.all_gather(latent_mod, "tp", axis=0, tiled=True)
    projected_rows = jnp.concatenate(
        [
            jnp.dot(piece, w_query, preferred_element_type=jnp.float32).astype(jnp.bfloat16),
            jnp.dot(piece, key_weight, preferred_element_type=jnp.float32).astype(jnp.bfloat16),
            jnp.dot(piece, value_weight, preferred_element_type=jnp.float32).astype(jnp.bfloat16),
        ],
        axis=1,
    )
    tokens_here = projected_rows.shape[0]
    kv_heads = kv_cols // HEAD_SIZE
    q_heads = q_cols // HEAD_SIZE
    query_group = q_heads // kv_heads
    offset = sp_index * tokens_here
    token_position = offset + jnp.arange(tokens_here, dtype=jnp.int32)
    query = axial_rotation(
        projected_rows[:, :q_cols].reshape(tokens_here, q_heads, HEAD_SIZE),
        token_position,
        GRID_WIDTH,
    )
    key = axial_rotation(
        projected_rows[:, q_cols : q_cols + kv_cols].reshape(tokens_here, kv_heads, HEAD_SIZE),
        token_position,
        GRID_WIDTH,
    )
    value_rows = projected_rows[:, q_cols + kv_cols :]
    extended = with_halo(
        jnp.concatenate([key.reshape(tokens_here, kv_cols), value_rows], axis=1),
        (("sp", 0),),
        WINDOW_SIDE,
    )
    block_list = tokens_here // WINDOW_SIDE
    band = jnp.concatenate(
        [
            extended[shift_index * WINDOW_SIDE : shift_index * WINDOW_SIDE + tokens_here].reshape(
                block_list, WINDOW_SIDE, 2 * kv_cols
            )
            for shift_index in range(3)
        ],
        axis=1,
    )
    band_key = band[..., :kv_cols].reshape(block_list, 3 * WINDOW_SIDE, kv_heads, HEAD_SIZE)
    band_value = band[..., kv_cols:].reshape(block_list, 3 * WINDOW_SIDE, kv_heads, HEAD_SIZE)
    context_key_rows = ctx_pair[:, :kv_cols].reshape(-1, kv_heads, HEAD_SIZE)
    context_value_rows = ctx_pair[:, kv_cols:].reshape(-1, kv_heads, HEAD_SIZE)
    query_block_list = query.reshape(block_list, WINDOW_SIDE, kv_heads, query_group, HEAD_SIZE)
    factor = HEAD_SIZE ** (-0.5)
    band_scores = (
        jnp.einsum(
            "nqhgd,nkhd->nhgqk", query_block_list, band_key, preferred_element_type=jnp.float32
        )
        * factor
    )
    total = tokens_here * sp_count
    qpos = token_position.reshape(block_list, WINDOW_SIDE)[:, :, None]
    kpos = (
        offset
        - WINDOW_SIDE
        + (jnp.arange(block_list, dtype=jnp.int32) * WINDOW_SIDE)[:, None, None]
        + jnp.arange(3 * WINDOW_SIDE, dtype=jnp.int32)[None, None, :]
    )
    valid = (jnp.abs(kpos - qpos) <= WINDOW_SIDE) & (kpos >= 0) & (kpos < total)
    band_scores = jnp.where(valid[:, None, None], band_scores, MASKED)
    ctx_scores = (
        jnp.einsum(
            "nqhgd,khd->nhgqk",
            query_block_list,
            context_key_rows,
            preferred_element_type=jnp.float32,
        )
        * factor
    )
    own_sink = lax.dynamic_slice_in_dim(sink, tp_index * q_heads, q_heads).reshape(
        kv_heads, query_group
    )[:, :, None, None]
    weights = sink_weights(jnp.concatenate([band_scores, ctx_scores], axis=-1), own_sink)
    attended = jnp.einsum(
        "nhgqk,nkhd->nqhgd",
        weights[..., : 3 * WINDOW_SIDE],
        band_value,
        preferred_element_type=jnp.float32,
    ) + jnp.einsum(
        "nhgqk,khd->nqhgd",
        weights[..., 3 * WINDOW_SIDE :],
        context_value_rows,
        preferred_element_type=jnp.float32,
    )
    attended = attended.astype(jnp.bfloat16).reshape(tokens_here, q_cols)
    projected = lax.psum_scatter(
        jnp.dot(attended, w_out, preferred_element_type=jnp.float32).astype(jnp.bfloat16),
        "tp",
        scatter_dimension=0,
        tiled=True,
    ).astype(jnp.float32)
    return (latent.astype(jnp.float32) + gate[0][None, :] * projected).astype(jnp.bfloat16)


def solution(mesh):
    in_specs = (
        P(("sp", "tp"), None),
        P("sp", None),
        P(),
        P(),
        P("sp", "tp"),
        P("sp", "tp"),
        P("sp", "tp"),
        P(None, "tp"),
        P(None, "tp"),
        P(None, "tp"),
        P("tp", None),
        P(),
    )
    out_specs = P(("sp", "tp"), None)
    return jax.shard_map(shards, mesh=mesh, in_specs=in_specs, out_specs=out_specs, check_vma=False)
```

profile of v0, /device:TPU:8, one launch (start us, length us, event | category | flops | bytes accessed | tf_op | source)
XLA Modules:
  0.0 172.2 jit_solution(11445464485622171272)
XLA Ops:
  6.5 0.9 fusion.49
  7.4 1.1 fusion.50
  8.5 1.0 convolution_bitcast_fusion.1
  9.6 1.0 convolution_bitcast_fusion.2
  10.6 0.9 broadcast_in_dim.12
  11.5 11.7 %all-to-all-start = ((f32[32,1,2560]{2,1,0:T(1,128)}), f32[32,1,2560]{2,1,0:T(1,128)}, u32[]{:S(2)}, u32[]{:S(2)}) async-start(f32[32,1,2560]{2,1,0:T(1,128)} %broadcast_in_dim.12), calls=%async_computation | async-start | bytes 655360 | tf_op jit(solution)/shard_map/all_to_all | solution.py:16
  23.3 1.2 convert_reduce_fusion
  24.6 1.3 fusion.10
  25.9 10.0 %all-to-all-done = f32[32,1,2560]{2,1,0:T(1,128)} async-done(((f32[32,1,2560]{2,1,0:T(1,128)}), f32[32,1,2560]{2,1,0:T(1,128)}, u32[]{:S(2)}, u32[]{:S(2)}) %all-to-all-start) | async-done | bytes 327712 | tf_op jit(solution)/shard_map/all_to_all | solution.py:16
  36.0 1.2 reduce_sum.54
  37.2 13.1 %all_gather.6 = f32[5,4096]{1,0:T(8,128)S(1)} all-gather(f32[5,512]{1,0:T(8,128)S(1)} %pad_maximum_fusion.4), channel_id=1, replica_groups=mesh['sp'=32,'tp'=8] {'tp'}, dimensions={1}, use_global_device_ids=true | all-gather | bytes 92160 | tf_op jit(solution)/shard_map/all_gather | solution.py:38
  50.4 2.1 %fusion.13 = bf16[64,4096]{1,0:T(8,128)(2,1)} fusion(bf16[64,4096]{1,0:T(8,128)(2,1)} %param.12, f32[4096]{0:T(1024)S(1)} %bitcast.140, f32[4096]{0:T(1024)S(1)} %bitcast.141, f32[64]{0:T(128)S(1)} %add_rsqrt_fusion.1, f32[64]{0:T(128)S(1)} %broadcast_multiply_fusion.1), kind=kLoop, calls=%fused_computation.30 | loop fusion | flops 1572864 | bytes 1081856 | tf_op jit(solution)/shard_map/convert_element_type | solution.py:136
  53.8 1.9 %fusion.16 = pred[4,128,384]{1,2,0:T(8,128)(4,1)} fusion(s32[4,128]{1,0:T(4,128)S(1)} %add_add_fusion, s32[4,384]{1,0:T(4,128)S(1)} %iota_add_fusion, pred[4,384]{1,0:T(4,128)(4,1)S(1)} %get-tuple-element.33, pred[4,384]{1,0:T(4,128)(4,1)S(1)} %get-tuple-element.32), kind=kLoop, calls=%fused_computation.36 | loop fusion | flops 983040 | bytes 207872 | tf_op jit(solution)/shard_map/and | solution.py:216
  55.7 1.2 multiply_cosine_fusion.1
  56.9 1.5 convolution_convert_fusion.4
  59.7 5.9 %all-to-all-start.1 = ((bf16[32,32,256]{2,1,0:T(8,128)(2,1)}), bf16[32,32,256]{2,1,0:T(8,128)(2,1)}, u32[]{:S(2)}, u32[]{:S(2)}) async-start(bf16[32,32,256]{2,1,0:T(8,128)(2,1)} %broadcast_in_dim.15), calls=%async_computation.1 | async-start | bytes 1048576 | tf_op jit(solution)/shard_map/all_to_all | solution.py:16
  65.6 17.7 %all-gather.2.cloned.1.call-done = bf16[512,4096]{1,0:T(8,128)(2,1)} async-done(((bf16[64,4096]{1,0:T(8,128)(2,1)}), bf16[512,4096]{1,0:T(8,128)(2,1)}) %all-gather.2.cloned.1.call-update) | async-done | bytes 4194320 | tf_op jit(solution)/shard_map/all_gather | solution.py:155
  83.3 3.7 %fusion.9 = f32[512,1,128]{0,2,1:T(8,128)S(1)} fusion(bf16[512,4096]{1,0:T(8,128)(2,1)} %all-gather.2.cloned.1.call-done, bf16[4096,128]{1,0:T(8,128)(2,1)S(1)} %copy-done.4), kind=kOutput, calls=%fused_computation.22 | convolution fusion | flops 537001984 | bytes 5505024 | tf_op jit(solution)/shard_map/dot_general | solution.py:159
  88.2 3.7 %convolution_convert_fusion.2 = bf16[512,128]{1,0:T(8,128)(2,1)S(1)} fusion(bf16[512,4096]{1,0:T(8,128)(2,1)} %all-gather.2.cloned.1.call-done, bf16[4096,128]{1,0:T(8,128)(2,1)} %param.21), kind=kOutput, calls=%fused_computation.19 | convolution fusion | flops 536936448 | bytes 5373952 | tf_op jit(solution)/shard_map/dot_general | solution.py:160
  92.9 3.4 %collective-permute-start = (bf16[128,256]{1,0:T(8,128)(2,1)}, bf16[128,256]{1,0:T(8,128)(2,1)}, u32[]{:S(2)}, u32[]{:S(2)}) collective-permute-start(bf16[128,256]{1,0:T(8,128)(2,1)} %get-tuple-element.19), channel_id=1, source_target_pairs={{0,8},{8,16},{16,24},{24,32},{32,40},{40,48},{48,56},{56,64},{64,7... | collective-permute-start | bytes 196616 | tf_op jit(solution)/shard_map/ppermute | solution.py:61
  96.3 3.3 %collective-permute-start.1 = (bf16[128,256]{1,0:T(8,128)(2,1)}, bf16[128,256]{1,0:T(8,128)(2,1)}, u32[]{:S(2)}, u32[]{:S(2)}) collective-permute-start(bf16[128,256]{1,0:T(8,128)(2,1)} %get-tuple-element.20), channel_id=1, source_target_pairs={{8,0},{16,8},{24,16},{32,24},{40,32},{48,40},{56,48},{64,56},{72,6... | collective-permute-start | bytes 196616 | tf_op jit(solution)/shard_map/ppermute | solution.py:63
  99.7 4.2 %convolution_convert_fusion.1 = bf16[512,256]{0,1:T(8,128)(2,1)S(1)} fusion(bf16[512,4096]{1,0:T(8,128)(2,1)} %all-gather.2.cloned.1.call-done, bf16[4096,256]{1,0:T(8,128)(2,1)} %param.19), kind=kOutput, calls=%fused_computation.17 | convolution fusion | flops 1073872896 | bytes 6553600 | tf_op jit(solution)/shard_map/dot_general | solution.py:158
  105.3 1.0 copy.68
  106.4 1.1 pad_maximum_fusion.3
  107.5 4.3 %fusion.59 = (f32[4,2,128]{2,1,0:T(2,128)}, f32[4,1,2,128,1024]{3,4,2,0,1:T(8,128)}) fusion(bf16[4,128,2,128]{3,1,2,0:T(8,128)(2,1)} %pad_maximum_fusion.3, bf16[1024,256]{1,0:T(8,128)(2,1)} %bitcast.31), kind=kOutput, calls=%fused_computation.123 | convolution fusion | flops 270531584 | bytes 4722688 | tf_op jit(solution)/shard_map/nqhgd,khd->nhgqk/dot_general | solution.py:219
  112.6 1.1 pad_maximum_fusion.2
  113.8 1.5 fusion.58
  116.2 1.0 divide_convert_fusion
  117.5 1.4 fusion.7
  119.2 3.2 %convolution_convert_fusion = bf16[512,4096]{1,0:T(8,128)(2,1)} fusion(bf16[256,4096]{1,0:T(8,128)(2,1)S(1)} %copy-done, bf16[64,8,2,128]{3,2,1,0:T(2,128)(2,1)S(1)} %bitcast.122), kind=kOutput, calls=%fused_computation | convolution fusion | flops 1075838976 | bytes 6553600 | tf_op jit(solution)/shard_map/dot_general | solution.py:244
  122.4 40.9 %reduce-scatter.2.cloned.1.call-done = bf16[64,4096]{1,0:T(8,128)(2,1)} async-done(((bf16[512,4096]{1,0:T(8,128)(2,1)}), bf16[64,4096]{1,0:T(8,128)(2,1)}) %reduce-scatter.2.cloned.1.call-update) | async-done | bytes 524304 | tf_op jit(solution)/shard_map/reduce_scatter | solution.py:243
  163.4 2.0 %fusion.14 = bf16[64,4096]{1,0:T(8,128)(2,1)} fusion(bf16[64,4096]{1,0:T(8,128)(2,1)S(1)} %copy-done.2, bf16[64,4096]{1,0:T(8,128)(2,1)} %reduce-scatter.2.cloned.1.call-done, f32[4096]{0:T(1024)S(1)} %bitcast.139), kind=kLoop, calls=%fused_computation.31 | loop fusion | flops 1310720 | bytes 1589248 | tf_op jit(solution)/shard_map/convert_element_type | solution.py:249
  (101 shorter events, 8.5 us)
Async XLA Ops:
  6.5 112.6 %copy-start = (bf16[256,4096]{1,0:T(8,128)(2,1)S(1)}, bf16[256,4096]{1,0:T(8,128)(2,1)}, u32[]{:S(2)}) copy-start(bf16[256,4096]{1,0:T(8,128)(2,1)} %param.22) | copy-start | bytes 6291460
  6.5 46.0 %copy-start.20 = (f32[16]{0:T(128)S(1)}, f32[16]{0:T(128)}, u32[]{:S(2)}) copy-start(f32[16]{0:T(128)} %param.23) | copy-start | bytes 196
  6.5 46.7 %copy-start.3 = (bf16[32,4096]{1,0:T(8,128)(2,1)S(1)}, bf16[32,4096]{1,0:T(8,128)(2,1)}, u32[]{:S(2)}) copy-start(bf16[32,4096]{1,0:T(8,128)(2,1)} %param.13) | copy-start | bytes 786436
  6.5 51.9 %copy-start.4 = (bf16[4096,128]{1,0:T(8,128)(2,1)S(1)}, bf16[4096,128]{1,0:T(8,128)(2,1)}, u32[]{:S(2)}) copy-start(bf16[4096,128]{1,0:T(8,128)(2,1)} %param.20) | copy-start | bytes 3145732
  11.5 24.4 %all-to-all-start = ((f32[32,1,2560]{2,1,0:T(1,128)}), f32[32,1,2560]{2,1,0:T(1,128)}, u32[]{:S(2)}, u32[]{:S(2)}) async-start(f32[32,1,2560]{2,1,0:T(1,128)} %broadcast_in_dim.12), calls=%async_computation | async-start | bytes 655360 | tf_op jit(solution)/shard_map/all_to_all | solution.py:16
  23.3 60.0 %all-gather.2.cloned.1.call-start = ((), (), s32[]{:S(2)}) async-start(), calls=%async_computation.3 | async-start | bytes 4718592 | tf_op jit(solution)/shard_map/all_gather | solution.py:155
  59.7 47.8 %all-to-all-start.1 = ((bf16[32,32,256]{2,1,0:T(8,128)(2,1)}), bf16[32,32,256]{2,1,0:T(8,128)(2,1)}, u32[]{:S(2)}, u32[]{:S(2)}) async-start(bf16[32,32,256]{2,1,0:T(8,128)(2,1)} %broadcast_in_dim.15), calls=%async_computation.1 | async-start | bytes 1048576 | tf_op jit(solution)/shard_map/all_to_all | solution.py:16
  65.6 97.8 %reduce-scatter.2.cloned.1.call-start = ((), (), s32[]{:S(2)}) async-start(), calls=%async_computation.4 | async-start | bytes 4718592 | tf_op jit(solution)/shard_map/reduce_scatter | solution.py:243
  87.6 0.6 copy-start.6
  87.6 0.6 copy-start.8
  87.6 0.6 copy-start.10
  87.6 0.6 copy-start.12
  92.9 19.7 %collective-permute-start = (bf16[128,256]{1,0:T(8,128)(2,1)}, bf16[128,256]{1,0:T(8,128)(2,1)}, u32[]{:S(2)}, u32[]{:S(2)}) collective-permute-start(bf16[128,256]{1,0:T(8,128)(2,1)} %get-tuple-element.19), channel_id=1, source_target_pairs={{0,8},{8,16},{16,24},{24,32},{32,40},{40,48},{48,56},{56,64},{64,7... | collective-permute-start | bytes 196616 | tf_op jit(solution)/shard_map/ppermute | solution.py:61
  96.3 7.6 %copy-start.14 = (f32[512,32]{0,1:T(8,128)S(1)}, f32[512,32]{0,1:T(8,128)}, u32[]{:S(2)}) copy-start(f32[512,32]{0,1:T(8,128)} %get-tuple-element.28) | copy-start | bytes 196612
  96.3 7.6 %copy-start.15 = (f32[512,32]{0,1:T(8,128)S(1)}, f32[512,32]{0,1:T(8,128)}, u32[]{:S(2)}) copy-start(f32[512,32]{0,1:T(8,128)} %get-tuple-element.29) | copy-start | bytes 196612
  96.3 7.6 %copy-start.16 = (f32[512,32]{0,1:T(8,128)S(1)}, f32[512,32]{0,1:T(8,128)}, u32[]{:S(2)}) copy-start(f32[512,32]{0,1:T(8,128)} %get-tuple-element.34) | copy-start | bytes 196612
  96.3 7.6 %copy-start.17 = (f32[512,32]{0,1:T(8,128)S(1)}, f32[512,32]{0,1:T(8,128)}, u32[]{:S(2)}) copy-start(f32[512,32]{0,1:T(8,128)} %get-tuple-element.35) | copy-start | bytes 196612
  96.3 16.3 %collective-permute-start.1 = (bf16[128,256]{1,0:T(8,128)(2,1)}, bf16[128,256]{1,0:T(8,128)(2,1)}, u32[]{:S(2)}, u32[]{:S(2)}) collective-permute-start(bf16[128,256]{1,0:T(8,128)(2,1)} %get-tuple-element.20), channel_id=1, source_target_pairs={{8,0},{16,8},{24,16},{32,24},{40,32},{48,40},{56,48},{64,56},{72,6... | collective-permute-start | bytes 196616 | tf_op jit(solution)/shard_map/ppermute | solution.py:63
  107.4 4.4 %copy-start.13 = (bf16[512,1,32]{0,2,1:T(8,128)(2,1)S(1)}, bf16[512,1,32]{0,2,1:T(8,128)(2,1)}, u32[]{:S(2)}) copy-start(bf16[512,1,32]{0,2,1:T(8,128)(2,1)} %copy-done.12) | copy-start | bytes 98308
  107.4 4.5 %copy-start.11 = (bf16[512,1,32]{0,2,1:T(8,128)(2,1)S(1)}, bf16[512,1,32]{0,2,1:T(8,128)(2,1)}, u32[]{:S(2)}) copy-start(bf16[512,1,32]{0,2,1:T(8,128)(2,1)} %copy-done.10) | copy-start | bytes 98308
  107.4 4.6 %copy-start.9 = (bf16[512,1,32]{0,2,1:T(8,128)(2,1)S(1)}, bf16[512,1,32]{0,2,1:T(8,128)(2,1)}, u32[]{:S(2)}) copy-start(bf16[512,1,32]{0,2,1:T(8,128)(2,1)} %copy-done.8) | copy-start | bytes 98308
  107.4 4.8 %copy-start.7 = (bf16[512,1,32]{0,2,1:T(8,128)(2,1)S(1)}, bf16[512,1,32]{0,2,1:T(8,128)(2,1)}, u32[]{:S(2)}) copy-start(bf16[512,1,32]{0,2,1:T(8,128)(2,1)} %copy-done.6) | copy-start | bytes 98308
  107.4 6.3 %copy-start.5 = (bf16[4,128,2,128]{3,1,2,0:T(8,128)(2,1)S(1)}, bf16[4,128,2,128]{3,1,2,0:T(8,128)(2,1)}, u32[]{:S(2)}) copy-start(bf16[4,128,2,128]{3,1,2,0:T(8,128)(2,1)} %pad_maximum_fusion.3) | copy-start | bytes 786436
  112.6 2.7 %copy-start.18 = (f32[4,2,128]{2,1,0:T(2,128)S(1)}, f32[4,2,128]{2,1,0:T(2,128)}, u32[]{:S(2)}) copy-start(f32[4,2,128]{2,1,0:T(2,128)} %get-tuple-element.38) | copy-start | bytes 12292
  112.6 2.7 %copy-start.19 = (f32[2]{0:T(128)S(1)}, f32[2]{0:T(128)}, u32[]{:S(2)}) copy-start(f32[2]{0:T(128)} %dynamic_slice.7) | copy-start | bytes 28
  112.6 2.7 %copy-start.1 = (f32[4,1,2,128,1024]{3,4,2,0,1:T(8,128)S(1)}, f32[4,1,2,128,1024]{3,4,2,0,1:T(8,128)}, u32[]{:S(2)}) copy-start(f32[4,1,2,128,1024]{3,4,2,0,1:T(8,128)} %get-tuple-element.39) | copy-start | bytes 12582916
  119.2 44.2 %copy-start.2 = (bf16[64,4096]{1,0:T(8,128)(2,1)S(1)}, bf16[64,4096]{1,0:T(8,128)(2,1)}, u32[]{:S(2)}) copy-start(bf16[64,4096]{1,0:T(8,128)(2,1)} %param.12) | copy-start | bytes 1572868
Sparse Core Ops, SparseCore 0:
  52.6 30.6 all-gather.1
  122.5 40.7 reduce-scatter.1
where the time goes:
time: 173 us; the launch traced here: 172 us
  waiting for transfers between devices  68.7 us (40%)
  matrix products  27.4 us (16%)
  starting transfers between devices  24.4 us (14%)
  other arithmetic  17.3 us (10%)
  between operations  14 us (8%)
  blocking collectives  13.1 us (8%)
  local copies, waits for them, and re-layouts  7.21 us (4%)
    reduce_scatter x1, waiting for transfers between devices, shards(): lax.psum_scatter(jnp.dot(attended, w_out, preferred_element_type=jnp.floa...  40.9 us
    all_gather x1, waiting for transfers between devices, shards(): piece = lax.all_gather(latent_mod, 'tp', axis=0, tiled=True)  17.7 us
    all_to_all x2, starting transfers between devices, sent_to_all(): lax.all_to_all(jnp.broadcast_to(value[None], (length, *value.shape)), axi...  17.6 us
    all_gather x1, blocking collectives, side_by_side(): filled = lax.all_gather(both, axis, axis=dim, tiled=True)  13.1 us
    all_to_all x2, waiting for transfers between devices, sent_to_all(): lax.all_to_all(jnp.broadcast_to(value[None], (length, *value.shape)), axi...  10 us
    dot_general x1, matrix products, shards(): jnp.einsum('nqhgd,khd->nhgqk', query_block_list, context_key_rows, prefer...  4.34 us
    dot_general x1, matrix products, shards(): jnp.dot(piece, w_query, preferred_element_type=jnp.float32)  4.16 us
    dot_general x1, matrix products, shards(): jnp.dot(piece, value_weight, preferred_element_type=jnp.float32)  3.73 us
  transfers between devices with their start and end apart: 6, of which 3 were waited for; matrix products, arithmetic and copies ran while one was open for 18% of the time, Pallas kernels for 0%

commit v1 on v0

--- a/solution.py
+++ b/solution.py
@@ -9,6 +9,12 @@
 EPS = 1e-05
 THETA = 10000.0
 MASKED = -1e30
+
+
+def joined_along(blocks, dim):
+    shape = list(blocks.shape[1:])
+    shape[dim] *= blocks.shape[0]
+    return jnp.moveaxis(blocks, 0, dim).reshape(shape)
 
 
 def sent_to_all(value, axis):
@@ -152,7 +158,19 @@
         "sp",
         0,
     )
-    piece = lax.all_gather(latent_mod, "tp", axis=0, tiled=True)
+    length_2 = lax.axis_size("tp")
+    pairs = [(i_2, (i_2 + 1) % length_2) for i_2 in range(length_2)]
+    back = [(b, a_2) for a_2, b in pairs]
+    lower, upper = ([], [])
+    for step in range(length_2 - 1):
+        if step % 2 == 0:
+            lower.append(lax.ppermute(lower[-1] if lower else latent_mod, "tp", pairs))
+        else:
+            upper.append(lax.ppermute(upper[-1] if upper else latent_mod, "tp", back))
+    tiles_2 = jnp.stack([*lower[::-1], latent_mod, *upper])
+    turn = lax.axis_index("tp") - len(lower)
+    tiles_2 = tiles_2[(jnp.arange(length_2) - turn) % length_2]
+    piece = joined_along(tiles_2, 0)
     projected_rows = jnp.concatenate(
         [
             jnp.dot(piece, w_query, preferred_element_type=jnp.float32).astype(jnp.bfloat16),

time: 173 us -> 221 us (1.28)
  local copies, waits for them, and re-layouts: 7.21 us -> 46.3 us
  starting transfers between devices: 24.4 us -> 32.7 us
  other arithmetic: 17.3 us -> 20.6 us
    ppermute x0 -> x7, waiting for transfers between devices: none -> 19.7 us  [the longest x4 19.7 us: shards(): lower.append(lax.ppermute(lower[-1] if lower else latent_mod, 'tp', pairs))]
    concatenate x16, local copies, waits for them, and re-layouts: 3.27 us -> 21.8 us  [axial_rotation(): jnp.concatenate([rotate_half(values[..., :width], token_position // grid,...]
    all_gather x1 -> x0, waiting for transfers between devices: 17.7 us -> none  [shards(): piece = lax.all_gather(latent_mod, 'tp', axis=0, tiled=True)]
    unnamed x44, local copies, waits for them, and re-layouts: 0.19 us -> 11.4 us
    ppermute x0 -> x7, starting transfers between devices: none -> 8.66 us  [the longest x3 8.3 us: shards(): upper.append(lax.ppermute(upper[-1] if upper else latent_mod, 'tp', back))]
    gather x0 -> x1, local copies, waits for them, and re-layouts: none -> 4.96 us  [shards(): tiles_2 = tiles_2[(jnp.arange(length_2) - turn) % length_2]]
    concatenate x2, local copies, waits for them, and re-layouts: 0.48 us -> 3.33 us  [shards(): jnp.concatenate([key.reshape(tokens_here, kv_cols), value_rows], axis=1)]
    dot_general x1, matrix products: 3.73 us -> 1.25 us  [shards(): jnp.dot(piece, value_weight, preferred_element_type=jnp.float32)]
  transfers between devices with their start and end apart: 6 -> 12, of which waited for: 3 -> 5; matrix products, arithmetic and copies ran while one was open for 18% -> 34% of each run, Pallas kernels for 0% -> 0%
where the time goes in v1:
time: 221 us; the launch traced here: 219 us
  waiting for transfers between devices  66.9 us (30%)
  local copies, waits for them, and re-layouts  46.3 us (21%)
  starting transfers between devices  32.7 us (15%)
  matrix products  25.5 us (12%)
  other arithmetic  20.6 us (9%)
  between operations  13.8 us (6%)
  blocking collectives  13.1 us (6%)
    reduce_scatter x1, waiting for transfers between devices, shards(): lax.psum_scatter(jnp.dot(attended, w_out, preferred_element_type=jnp.floa...  39.5 us
    concatenate x16, local copies, waits for them, and re-layouts, axial_rotation(): jnp.concatenate([rotate_half(values[..., :width], token_position // grid,...  21.8 us
    ppermute x4, waiting for transfers between devices, shards(): lower.append(lax.ppermute(lower[-1] if lower else latent_mod, 'tp', pairs))  19.7 us
    all_to_all x2, starting transfers between devices, sent_to_all(): lax.all_to_all(jnp.broadcast_to(value[None], (length, *value.shape)), axi...  17.3 us
    all_gather x1, blocking collectives, side_by_side(): filled = lax.all_gather(both, axis, axis=dim, tiled=True)  13.1 us
    unnamed x44, local copies, waits for them, and re-layouts  11.4 us
    ppermute x3, starting transfers between devices, shards(): upper.append(lax.ppermute(upper[-1] if upper else latent_mod, 'tp', back))  8.3 us
    all_to_all x2, waiting for transfers between devices, sent_to_all(): lax.all_to_all(jnp.broadcast_to(value[None], (length, *value.shape)), axi...  7.61 us
  transfers between devices with their start and end apart: 12, of which 5 were waited for; matrix products, arithmetic and copies ran while one was open for 34% of the time, Pallas kernels for 0%

profile of v1, /device:TPU:8, one launch (start us, length us, event | category | flops | bytes accessed | tf_op | source)
XLA Modules:
  0.0 218.9 jit_solution(7625388339555118393)
XLA Ops:
  11.5 11.7 %all-to-all-start = ((f32[32,1,2560]{2,1,0:T(1,128)}), f32[32,1,2560]{2,1,0:T(1,128)S(1)}, u32[]{:S(2)}, u32[]{:S(2)}) async-start(f32[32,1,2560]{2,1,0:T(1,128)} %broadcast_in_dim.12), calls=%async_computation | async-start | bytes 655360 | tf_op jit(solution)/shard_map/all_to_all | solution.py:22
  28.2 7.6 %all-to-all-done = f32[32,1,2560]{2,1,0:T(1,128)S(1)} async-done(((f32[32,1,2560]{2,1,0:T(1,128)}), f32[32,1,2560]{2,1,0:T(1,128)S(1)}, u32[]{:S(2)}, u32[]{:S(2)}) %all-to-all-start) | async-done | bytes 327712 | tf_op jit(solution)/shard_map/all_to_all | solution.py:22
  36.1 13.1 %all_gather.3 = f32[5,4096]{1,0:T(8,128)S(1)} all-gather(f32[5,512]{1,0:T(8,128)S(1)} %pad_maximum_fusion.4), channel_id=1, replica_groups=mesh['sp'=32,'tp'=8] {'tp'}, dimensions={1}, use_global_device_ids=true | all-gather | bytes 92160 | tf_op jit(solution)/shard_map/all_gather | solution.py:44
  51.2 9.2 %collective-permute-done = bf16[64,4096]{1,0:T(8,128)(2,1)S(1)} collective-permute-done((bf16[64,4096]{1,0:T(8,128)(2,1)S(1)}, bf16[64,4096]{1,0:T(8,128)(2,1)S(1)}, u32[]{:S(2)}, u32[]{:S(2)}) %collective-permute-start) | collective-permute-done | bytes 524320 | tf_op jit(solution)/shard_map/ppermute | solution.py:167
  60.5 3.0 %collective-permute-start.4 = (bf16[64,4096]{1,0:T(8,128)(2,1)S(1)}, bf16[64,4096]{1,0:T(8,128)(2,1)}, u32[]{:S(2)}, u32[]{:S(2)}) collective-permute-start(bf16[64,4096]{1,0:T(8,128)(2,1)S(1)} %fusion.13), channel_id=1, source_target_pairs={{1,0},{2,1},{3,2},{4,3},{5,4},{6,5},{7,6},{0,7},{9,8},{10,9},{11,1... | collective-permute-start | bytes 1572872 | tf_op jit(solution)/shard_map/ppermute | solution.py:169
  63.5 6.7 %collective-permute-done.1 = bf16[64,4096]{1,0:T(8,128)(2,1)S(1)} collective-permute-done((bf16[64,4096]{1,0:T(8,128)(2,1)S(1)}, bf16[64,4096]{1,0:T(8,128)(2,1)S(1)}, u32[]{:S(2)}, u32[]{:S(2)}) %collective-permute-start.1) | collective-permute-done | bytes 524320 | tf_op jit(solution)/shard_map/ppermute | solution.py:167
  70.2 1.9 fusion.16
  73.3 2.9 %collective-permute-start.5 = (bf16[64,4096]{1,0:T(8,128)(2,1)}, bf16[64,4096]{1,0:T(8,128)(2,1)}, u32[]{:S(2)}, u32[]{:S(2)}) collective-permute-start(bf16[64,4096]{1,0:T(8,128)(2,1)} %collective-permute-done.4), channel_id=1, source_target_pairs={{1,0},{2,1},{3,2},{4,3},{5,4},{6,5},{7,6},{0,7},{9,8},{10,9},{11,1... | collective-permute-start | bytes 1572872 | tf_op jit(solution)/shard_map/ppermute | solution.py:169
  76.3 3.8 %collective-permute-done.2 = bf16[64,4096]{1,0:T(8,128)(2,1)} collective-permute-done((bf16[64,4096]{1,0:T(8,128)(2,1)S(1)}, bf16[64,4096]{1,0:T(8,128)(2,1)}, u32[]{:S(2)}, u32[]{:S(2)}) %collective-permute-start.2) | collective-permute-done | bytes 524320 | tf_op jit(solution)/shard_map/ppermute | solution.py:167
  84.2 5.6 %all-to-all-start.1 = ((bf16[32,32,256]{2,1,0:T(8,128)(2,1)}), bf16[32,32,256]{2,1,0:T(8,128)(2,1)S(1)}, u32[]{:S(2)}, u32[]{:S(2)}) async-start(bf16[32,32,256]{2,1,0:T(8,128)(2,1)} %broadcast_in_dim.15), calls=%async_computation.1 | async-start | bytes 1048576 | tf_op jit(solution)/shard_map/all_to_all | solution.py:22
  89.8 2.4 %collective-permute-start.6 = (bf16[64,4096]{1,0:T(8,128)(2,1)}, bf16[64,4096]{1,0:T(8,128)(2,1)S(1)}, u32[]{:S(2)}, u32[]{:S(2)}) collective-permute-start(bf16[64,4096]{1,0:T(8,128)(2,1)} %collective-permute-done.5), channel_id=1, source_target_pairs={{1,0},{2,1},{3,2},{4,3},{5,4},{6,5},{7,6},{0,7},{9,8},{10,9},{11,1... | collective-permute-start | bytes 1572872 | tf_op jit(solution)/shard_map/ppermute | solution.py:169
  92.3 1.9 bitcast_dynamic-update-slice_fusion.7
  94.1 1.9 bitcast_dynamic-update-slice_fusion.6
  96.0 1.9 bitcast_dynamic-update-slice_fusion.5
  97.9 1.9 bitcast_dynamic-update-slice_fusion.4
  100.9 1.9 bitcast_dynamic-update-slice_fusion.2
  102.7 1.9 bitcast_dynamic-update-slice_fusion.1
  105.5 5.0 %gather_fusion = bf16[8,64,4096]{2,1,0:T(8,128)(2,1)} fusion(bf16[8,64,4096]{2,1,0:T(8,128)(2,1)} %bitcast_dynamic-update-slice_fusion, s32[1024]{0:T(1024)S(1)} %pad_clamp_fusion), kind=kCustom, calls=%fused_computation | custom fusion | bytes 8388640 | tf_op jit(solution)/shard_map/gather | solution.py:172
  110.4 4.1 %fusion.9 = f32[512,1,128]{0,2,1:T(8,128)S(1)} fusion(bf16[512,4096]{1,0:T(8,128)(2,1)} %bitcast.141, bf16[4096,128]{1,0:T(8,128)(2,1)} %param.20), kind=kOutput, calls=%fused_computation.23 | convolution fusion | flops 537001984 | bytes 5505024 | tf_op jit(solution)/shard_map/dot_general | solution.py:177
  121.5 3.4 %collective-permute-start.7 = (bf16[128,256]{1,0:T(8,128)(2,1)}, bf16[128,256]{1,0:T(8,128)(2,1)}, u32[]{:S(2)}, u32[]{:S(2)}) collective-permute-start(bf16[128,256]{1,0:T(8,128)(2,1)} %get-tuple-element.19), channel_id=1, source_target_pairs={{0,8},{8,16},{16,24},{24,32},{32,40},{40,48},{48,56},{56,64},{64,7... | collective-permute-start | bytes 196616 | tf_op jit(solution)/shard_map/ppermute | solution.py:67
  124.9 3.4 %collective-permute-start.8 = (bf16[128,256]{1,0:T(8,128)(2,1)}, bf16[128,256]{1,0:T(8,128)(2,1)}, u32[]{:S(2)}, u32[]{:S(2)}) collective-permute-start(bf16[128,256]{1,0:T(8,128)(2,1)} %get-tuple-element.20), channel_id=1, source_target_pairs={{8,0},{16,8},{24,16},{32,24},{40,32},{48,40},{56,48},{64,56},{72,6... | collective-permute-start | bytes 196616 | tf_op jit(solution)/shard_map/ppermute | solution.py:69
  128.3 4.2 %convolution_convert_fusion.1 = bf16[512,256]{0,1:T(8,128)(2,1)S(1)} fusion(bf16[512,4096]{1,0:T(8,128)(2,1)} %bitcast.142, bf16[4096,256]{1,0:T(8,128)(2,1)} %param.19), kind=kOutput, calls=%fused_computation.18 | convolution fusion | flops 1073872896 | bytes 6553600 | tf_op jit(solution)/shard_map/dot_general | solution.py:176
  134.8 1.7 copy.68
  138.0 1.7 copy.69
  141.2 1.7 copy.70
  144.4 1.7 copy.71
  146.1 2.2 %pad_maximum_fusion.3 = bf16[4,128,2,128]{3,1,2,0:T(8,128)(2,1)} fusion(bf16[4,128,2,32]{3,1,2,0:T(8,128)(2,1)} %copy.71, bf16[4,128,2,32]{3,1,2,0:T(8,128)(2,1)} %copy.70, bf16[4,128,2,32]{3,1,2,0:T(8,128)(2,1)} %copy.69, bf16[4,128,2,32]{3,1,2,0:T(8,128)(2,1)} %copy.68), kind=kLoop, calls=%fused_computation.62 | loop fusion | flops 1048576 | bytes 524288 | tf_op jit(solution)/shard_map/concatenate | solution.py:99
  148.3 4.2 %fusion.61 = (f32[4,2,128]{2,1,0:T(2,128)}, f32[4,1,2,128,1024]{3,4,2,0,1:T(8,128)}) fusion(bf16[4,128,2,128]{3,1,2,0:T(8,128)(2,1)} %pad_maximum_fusion.3, bf16[1024,256]{1,0:T(8,128)(2,1)S(1)} %bitcast.144), kind=kOutput, calls=%fused_computation.139 | convolution fusion | flops 270531584 | bytes 4722688 | tf_op jit(solution)/shard_map/nqhgd,khd->nhgqk/dot_general | solution.py:237
  158.6 2.0 concatenate.95
  167.3 3.2 %convolution_convert_fusion = bf16[512,4096]{1,0:T(8,128)(2,1)} fusion(bf16[256,4096]{1,0:T(8,128)(2,1)S(1)} %copy-done, bf16[64,8,2,128]{3,2,1,0:T(2,128)(2,1)S(1)} %bitcast.146), kind=kOutput, calls=%fused_computation.1 | convolution fusion | flops 1075838976 | bytes 6553600 | tf_op jit(solution)/shard_map/dot_general | solution.py:262
  170.5 39.5 %reduce-scatter.2.cloned.1.call-done = bf16[64,4096]{1,0:T(8,128)(2,1)} async-done(((bf16[512,4096]{1,0:T(8,128)(2,1)}), bf16[64,4096]{1,0:T(8,128)(2,1)}) %reduce-scatter.2.cloned.1.call-update) | async-done | bytes 524304 | tf_op jit(solution)/shard_map/reduce_scatter | solution.py:261
  210.1 2.0 fusion.14
  (117 shorter events, 45.9 us)
Async XLA Ops:
  6.5 160.8 %copy-start = (bf16[256,4096]{1,0:T(8,128)(2,1)S(1)}, bf16[256,4096]{1,0:T(8,128)(2,1)}, u32[]{:S(2)}) copy-start(bf16[256,4096]{1,0:T(8,128)(2,1)} %param.22) | copy-start | bytes 6291460
  6.5 44.4 %copy-start.4 = (bf16[32,4096]{1,0:T(8,128)(2,1)S(1)}, bf16[32,4096]{1,0:T(8,128)(2,1)}, u32[]{:S(2)}) copy-start(bf16[32,4096]{1,0:T(8,128)(2,1)} %param.13) | copy-start | bytes 786436
  11.5 24.3 %all-to-all-start = ((f32[32,1,2560]{2,1,0:T(1,128)}), f32[32,1,2560]{2,1,0:T(1,128)S(1)}, u32[]{:S(2)}, u32[]{:S(2)}) async-start(f32[32,1,2560]{2,1,0:T(1,128)} %broadcast_in_dim.12), calls=%async_computation | async-start | bytes 655360 | tf_op jit(solution)/shard_map/all_to_all | solution.py:22
  50.5 9.8 %collective-permute-start = (bf16[64,4096]{1,0:T(8,128)(2,1)S(1)}, bf16[64,4096]{1,0:T(8,128)(2,1)S(1)}, u32[]{:S(2)}, u32[]{:S(2)}) collective-permute-start(bf16[64,4096]{1,0:T(8,128)(2,1)S(1)} %fusion.13), channel_id=1, source_target_pairs={{0,1},{1,2},{2,3},{3,4},{4,5},{5,6},{6,7},{7,0},{8,9},{9,10},{10,1... | collective-permute-start | bytes 1572872 | tf_op jit(solution)/shard_map/ppermute | solution.py:167
  60.4 22.9 %copy-start.6 = (bf16[64,4096]{1,0:T(8,128)(2,1)}, bf16[64,4096]{1,0:T(8,128)(2,1)S(1)}, u32[]{:S(2)}) copy-start(bf16[64,4096]{1,0:T(8,128)(2,1)S(1)} %collective-permute-done) | copy-start | bytes 1572868
  60.4 9.8 %collective-permute-start.1 = (bf16[64,4096]{1,0:T(8,128)(2,1)S(1)}, bf16[64,4096]{1,0:T(8,128)(2,1)S(1)}, u32[]{:S(2)}, u32[]{:S(2)}) collective-permute-start(bf16[64,4096]{1,0:T(8,128)(2,1)S(1)} %collective-permute-done), channel_id=1, source_target_pairs={{0,1},{1,2},{2,3},{3,4},{4,5},{5,6},{6,7},{7,0},{8,9},{9,10},{10,1... | collective-permute-start | bytes 1572872 | tf_op jit(solution)/shard_map/ppermute | solution.py:167
  60.5 12.8 %collective-permute-start.4 = (bf16[64,4096]{1,0:T(8,128)(2,1)S(1)}, bf16[64,4096]{1,0:T(8,128)(2,1)}, u32[]{:S(2)}, u32[]{:S(2)}) collective-permute-start(bf16[64,4096]{1,0:T(8,128)(2,1)S(1)} %fusion.13), channel_id=1, source_target_pairs={{1,0},{2,1},{3,2},{4,3},{5,4},{6,5},{7,6},{0,7},{9,8},{10,9},{11,1... | collective-permute-start | bytes 1572872 | tf_op jit(solution)/shard_map/ppermute | solution.py:169
  70.2 13.1 %copy-start.7 = (bf16[64,4096]{1,0:T(8,128)(2,1)}, bf16[64,4096]{1,0:T(8,128)(2,1)S(1)}, u32[]{:S(2)}) copy-start(bf16[64,4096]{1,0:T(8,128)(2,1)S(1)} %collective-permute-done.1) | copy-start | bytes 1572868
  70.2 9.9 %collective-permute-start.2 = (bf16[64,4096]{1,0:T(8,128)(2,1)S(1)}, bf16[64,4096]{1,0:T(8,128)(2,1)}, u32[]{:S(2)}, u32[]{:S(2)}) collective-permute-start(bf16[64,4096]{1,0:T(8,128)(2,1)S(1)} %collective-permute-done.1), channel_id=1, source_target_pairs={{0,1},{1,2},{2,3},{3,4},{4,5},{5,6},{6,7},{7,0},{8,9},{9,10},{10,1... | collective-permute-start | bytes 1572872 | tf_op jit(solution)/shard_map/ppermute | solution.py:167
  73.3 16.5 %collective-permute-start.5 = (bf16[64,4096]{1,0:T(8,128)(2,1)}, bf16[64,4096]{1,0:T(8,128)(2,1)}, u32[]{:S(2)}, u32[]{:S(2)}) collective-permute-start(bf16[64,4096]{1,0:T(8,128)(2,1)} %collective-permute-done.4), channel_id=1, source_target_pairs={{1,0},{2,1},{3,2},{4,3},{5,4},{6,5},{7,6},{0,7},{9,8},{10,9},{11,1... | collective-permute-start | bytes 1572872 | tf_op jit(solution)/shard_map/ppermute | solution.py:169
  80.1 12.1 %collective-permute-start.3 = (bf16[64,4096]{1,0:T(8,128)(2,1)}, bf16[64,4096]{1,0:T(8,128)(2,1)}, u32[]{:S(2)}, u32[]{:S(2)}) collective-permute-start(bf16[64,4096]{1,0:T(8,128)(2,1)} %collective-permute-done.2), channel_id=1, source_target_pairs={{0,1},{1,2},{2,3},{3,4},{4,5},{5,6},{6,7},{7,0},{8,9},{9,10},{10,1... | collective-permute-start | bytes 1572872 | tf_op jit(solution)/shard_map/ppermute | solution.py:167
  80.1 19.7 %copy-start.3 = (bf16[64,4096]{1,0:T(8,128)(2,1)S(1)}, bf16[64,4096]{1,0:T(8,128)(2,1)}, u32[]{:S(2)}) copy-start(bf16[64,4096]{1,0:T(8,128)(2,1)} %param.12) | copy-start | bytes 1572868
  84.2 64.1 %all-to-all-start.1 = ((bf16[32,32,256]{2,1,0:T(8,128)(2,1)}), bf16[32,32,256]{2,1,0:T(8,128)(2,1)S(1)}, u32[]{:S(2)}, u32[]{:S(2)}) async-start(bf16[32,32,256]{2,1,0:T(8,128)(2,1)} %broadcast_in_dim.15), calls=%async_computation.1 | async-start | bytes 1048576 | tf_op jit(solution)/shard_map/all_to_all | solution.py:22
  89.8 120.3 %reduce-scatter.2.cloned.1.call-start = ((), (), s32[]{:S(2)}) async-start(), calls=%async_computation.3 | async-start | bytes 4718592 | tf_op jit(solution)/shard_map/reduce_scatter | solution.py:261
  89.8 14.8 %collective-permute-start.6 = (bf16[64,4096]{1,0:T(8,128)(2,1)}, bf16[64,4096]{1,0:T(8,128)(2,1)S(1)}, u32[]{:S(2)}, u32[]{:S(2)}) collective-permute-start(bf16[64,4096]{1,0:T(8,128)(2,1)} %collective-permute-done.5), channel_id=1, source_target_pairs={{1,0},{2,1},{3,2},{4,3},{5,4},{6,5},{7,6},{0,7},{9,8},{10,9},{11,1... | collective-permute-start | bytes 1572872 | tf_op jit(solution)/shard_map/ppermute | solution.py:169
  110.4 4.2 %copy-start.2 = (bf16[8,64,4096]{2,1,0:T(8,128)(2,1)S(1)}, bf16[8,64,4096]{2,1,0:T(8,128)(2,1)}, u32[]{:S(2)}) copy-start(bf16[8,64,4096]{2,1,0:T(8,128)(2,1)} %gather_fusion) | copy-start | bytes 12582916
  110.4 4.2 %copy-start.5 = (bf16[4096,128]{1,0:T(8,128)(2,1)S(1)}, bf16[4096,128]{1,0:T(8,128)(2,1)}, u32[]{:S(2)}) copy-start(bf16[4096,128]{1,0:T(8,128)(2,1)} %param.21) | copy-start | bytes 3145732
  116.4 2.3 %copy-start.8 = (bf16[512,1,32]{0,2,1:T(8,128)(2,1)}, bf16[512,1,32]{0,2,1:T(8,128)(2,1)S(1)}, u32[]{:S(2)}) copy-start(bf16[512,1,32]{0,2,1:T(8,128)(2,1)S(1)} %get-tuple-element.11) | copy-start | bytes 98308
  116.4 2.3 %copy-start.9 = (bf16[512,1,32]{0,2,1:T(8,128)(2,1)}, bf16[512,1,32]{0,2,1:T(8,128)(2,1)S(1)}, u32[]{:S(2)}) copy-start(bf16[512,1,32]{0,2,1:T(8,128)(2,1)S(1)} %get-tuple-element.12) | copy-start | bytes 98308
  116.5 2.3 %copy-start.10 = (bf16[512,1,32]{0,2,1:T(8,128)(2,1)}, bf16[512,1,32]{0,2,1:T(8,128)(2,1)S(1)}, u32[]{:S(2)}) copy-start(bf16[512,1,32]{0,2,1:T(8,128)(2,1)S(1)} %get-tuple-element.16) | copy-start | bytes 98308
  116.5 2.3 %copy-start.11 = (bf16[512,1,32]{0,2,1:T(8,128)(2,1)}, bf16[512,1,32]{0,2,1:T(8,128)(2,1)S(1)}, u32[]{:S(2)}) copy-start(bf16[512,1,32]{0,2,1:T(8,128)(2,1)S(1)} %get-tuple-element.15) | copy-start | bytes 98308
  121.5 39.1 %collective-permute-start.7 = (bf16[128,256]{1,0:T(8,128)(2,1)}, bf16[128,256]{1,0:T(8,128)(2,1)}, u32[]{:S(2)}, u32[]{:S(2)}) collective-permute-start(bf16[128,256]{1,0:T(8,128)(2,1)} %get-tuple-element.19), channel_id=1, source_target_pairs={{0,8},{8,16},{16,24},{24,32},{32,40},{40,48},{48,56},{56,64},{64,7... | collective-permute-start | bytes 196616 | tf_op jit(solution)/shard_map/ppermute | solution.py:67
  124.9 7.6 %copy-start.12 = (f32[512,32]{0,1:T(8,128)S(1)}, f32[512,32]{0,1:T(8,128)}, u32[]{:S(2)}) copy-start(f32[512,32]{0,1:T(8,128)} %get-tuple-element.28) | copy-start | bytes 196612
  124.9 7.6 %copy-start.13 = (f32[512,32]{0,1:T(8,128)S(1)}, f32[512,32]{0,1:T(8,128)}, u32[]{:S(2)}) copy-start(f32[512,32]{0,1:T(8,128)} %get-tuple-element.29) | copy-start | bytes 196612
  124.9 7.6 %copy-start.14 = (f32[512,32]{0,1:T(8,128)S(1)}, f32[512,32]{0,1:T(8,128)}, u32[]{:S(2)}) copy-start(f32[512,32]{0,1:T(8,128)} %get-tuple-element.34) | copy-start | bytes 196612
  124.9 7.6 %copy-start.15 = (f32[512,32]{0,1:T(8,128)S(1)}, f32[512,32]{0,1:T(8,128)}, u32[]{:S(2)}) copy-start(f32[512,32]{0,1:T(8,128)} %get-tuple-element.35) | copy-start | bytes 196612
  124.9 35.7 %collective-permute-start.8 = (bf16[128,256]{1,0:T(8,128)(2,1)}, bf16[128,256]{1,0:T(8,128)(2,1)}, u32[]{:S(2)}, u32[]{:S(2)}) collective-permute-start(bf16[128,256]{1,0:T(8,128)(2,1)} %get-tuple-element.20), channel_id=1, source_target_pairs={{8,0},{16,8},{24,16},{32,24},{40,32},{48,40},{56,48},{64,56},{72,6... | collective-permute-start | bytes 196616 | tf_op jit(solution)/shard_map/ppermute | solution.py:69
  160.6 3.7 %copy-start.16 = (f32[4,2,128]{2,1,0:T(2,128)S(1)}, f32[4,2,128]{2,1,0:T(2,128)}, u32[]{:S(2)}) copy-start(f32[4,2,128]{2,1,0:T(2,128)} %get-tuple-element.38) | copy-start | bytes 12292
  160.6 3.8 %copy-start.17 = (f32[2]{0:T(128)S(1)}, f32[2]{0:T(128)}, u32[]{:S(2)}) copy-start(f32[2]{0:T(128)} %dynamic_slice.7) | copy-start | bytes 28
  160.6 3.8 %copy-start.1 = (f32[4,1,2,128,1024]{3,4,2,0,1:T(8,128)S(1)}, f32[4,1,2,128,1024]{3,4,2,0,1:T(8,128)}, u32[]{:S(2)}) copy-start(f32[4,1,2,128,1024]{3,4,2,0,1:T(8,128)} %get-tuple-element.39) | copy-start | bytes 12582916
Sparse Core Ops, SparseCore 0:
  170.7 39.3 reduce-scatter.1
